TPU v7x, 32 devices: a whole 2x2x4 slice. The times are simulated.
32 devices in a mesh: grp: 2 (over y), ep: 4 (over z), tp: 4 (over x, core).
Axes of the slice: x: 2, y: 2, z: 4, core: 2. Of those that a mesh axis runs over, the one named last changes fastest.
Arguments:
- hidden_in: bfloat16 [4096, 2048], P(('grp', 'ep', 'tp')), parts along dimension 0, may hold values from -6 to 6
- expert_ids: int32 [4096, 2], P(('grp', 'ep', 'tp')), parts along dimension 0, may hold values from 0 to 15, all different within a row; in each aligned block of 128 rows (0 to 127, 128 to 255, ...) at most 32 rows name the same one
- route_weights: float32 [4096, 2], P(('grp', 'ep', 'tp')), parts along dimension 0, may hold values from 0.1 to 1
- norm_gain: float32 [2048], replicated, may hold values from 0.1 to 1.9
- gate_proj: bfloat16 [16, 2048, 512], P(('ep', 'tp')), may hold values from -0.125 to 0.125
- up_proj: bfloat16 [16, 2048, 512], P(('ep', 'tp')), may hold values from -0.125 to 0.125
- down_proj: bfloat16 [16, 512, 2048], P(('ep', 'tp')), may hold values from -0.25 to 0.25
Outputs:
- mixed_out: bfloat16 [4096, 2048], P(('grp', 'ep', 'tp')), parts along dimension 0
There are 2 independent parts, one for each index of `grp`. A program takes and returns all parts, laid end to end along the dimension named above; an argument that names none is the same for every part. Nothing has to cross between parts.
Inputs may be any that keep to these rules, and one draw needn't show every extreme that they name: `expert_ids`: each token names 2 different experts; among the 128 tokens of one device (aligned blocks of rows) no expert is named more than 32 times, and in every draw some expert is named exactly 32 times by some device's tokens.
All inputs are finite; a program needn't handle non-finite values.
Results may differ from a plain program's by a relative error of at most 0.0071.
Values may be sent and summed in bfloat16 or wider, within the bound.
A program may use at most 64 MiB of HBM per device.

v0:
```python
import jax
import jax.numpy as jnp
from jax import lax
from jax.sharding import PartitionSpec as P


def body(hidden_in, expert_ids, route_weights, norm_gain, gate_proj, up_proj, down_proj):
    token_count = hidden_in.shape[0]
    model_width = hidden_in.shape[1]
    choose_count = expert_ids.shape[1]
    ep_count = lax.axis_size("ep")
    tp_count = lax.axis_size("tp")
    expert_count = ep_count * tp_count
    capacity = max(2, 2 * choose_count * token_count // expert_count)
    as_float = hidden_in.astype(jnp.float32)
    scaled = as_float * lax.rsqrt(jnp.mean(as_float * as_float, axis=-1, keepdims=True) + 1e-06)
    normed = (scaled * norm_gain).astype(jnp.bfloat16)
    flat_ids = expert_ids.reshape(-1)
    onehot = (flat_ids[:, None] == jnp.arange(expert_count, dtype=jnp.int32)[None, :]).astype(
        jnp.int32
    )
    slot_index = jnp.sum((jnp.cumsum(onehot, axis=0) - onehot) * onehot, axis=1)
    target = flat_ids * capacity + slot_index
    routed = jnp.repeat(normed, choose_count, axis=0)
    buffer = jnp.zeros((expert_count * capacity, model_width), jnp.bfloat16).at[target].set(routed)
    buffer = buffer.reshape(expert_count, capacity, model_width)
    arrived = lax.all_to_all(buffer, ("ep", "tp"), split_axis=0, concat_axis=0, tiled=True)
    shape_in = arrived.shape
    block_in = arrived.reshape(-1, model_width)
    gate_act = jnp.dot(block_in, gate_proj[0], preferred_element_type=jnp.float32)
    up_act = jnp.dot(block_in, up_proj[0], preferred_element_type=jnp.float32)
    hidden = (jax.nn.silu(gate_act) * up_act).astype(jnp.bfloat16)
    result = jnp.dot(hidden, down_proj[0], preferred_element_type=jnp.float32).astype(jnp.bfloat16)
    results = result.reshape(shape_in)
    returned = lax.all_to_all(results, ("ep", "tp"), split_axis=0, concat_axis=0, tiled=True)
    picked = returned.reshape(-1, model_width)[target].astype(jnp.float32)
    picked = picked.reshape(token_count, choose_count, model_width)
    return jnp.sum(picked * route_weights[:, :, None], axis=1).astype(jnp.bfloat16)


def solution(mesh):
    return jax.shard_map(
        body,
        mesh=mesh,
        in_specs=(
            P(("grp", "ep", "tp"), None),
            P(("grp", "ep", "tp"), None),
            P(("grp", "ep", "tp"), None),
            P(),
            P(("ep", "tp"), None, None),
            P(("ep", "tp"), None, None),
            P(("ep", "tp"), None, None),
        ),
        out_specs=P(("grp", "ep", "tp"), None),
        check_vma=False,
    )
```

profile of v0, /device:TPU:11, one launch (start us, length us, event | category | flops | bytes accessed | tf_op | source)
XLA Modules:
  0.0 139.3 jit_solution(16366005023959419473)
XLA Ops:
  0.0 0.9 copy.10
  0.9 0.1 eq.29
  1.1 0.1 eq.25
  1.2 0.7 broadcast_multiply_fusion
  1.9 0.6 reduce-window.6
  2.5 0.2 slice_reduce_fusion
  2.7 0.1 copy.9
  2.8 0.1 mul.55
  3.0 1.2 fusion.11
  4.2 1.2 fusion.13
  5.5 0.6 broadcast_in_dim.5
  6.1 1.2 reshape.94
  7.3 0.1 fusion.21
  7.4 4.4 %scatter_custom_fusion = bf16[512,2048]{1,0:T(8,128)(2,1)} fusion(s32[256]{0:T(256)S(1)} %bitcast.46, bf16[256,2048]{1,0:T(8,128)(2,1)} %reshape.94, bf16[]{:T(256)} %constant.8.clone.1), kind=kCustom, calls=%fused_computation.16 | custom fusion | bytes 2097664 | tf_op jit(solution)/shard_map/scatter | solution.py:25
  11.9 53.9 %all_to_all.10 = bf16[16,32,2048]{2,1,0:T(8,128)(2,1)S(1)} all-to-all(bf16[16,32,2048]{2,1,0:T(8,128)(2,1)} %bitcast.42), channel_id=1, replica_groups=mesh['grp'=2,'ep'=4,'tp'=4] {'ep','tp'}, dimensions={0} | all-to-all | bytes 4194304 | tf_op jit(solution)/shard_map/all_to_all | solution.py:27
  65.8 1.3 copy-done.1
  67.1 1.2 fusion.3
  68.3 6.1 %convolution_convert_fusion = bf16[512,2048]{1,0:T(8,128)(2,1)} fusion(bf16[1,512,2048]{2,1,0:T(8,128)(2,1)S(1)} %copy-done, bf16[512,2048]{1,0:T(8,128)(2,1)} %bitcast.45, bf16[1,2048,512]{2,1,0:T(8,128)(2,1)} %param.12, f32[512,512]{1,0:T(8,128)S(1)} %fusion.3), kind=kOutput, calls=%fused_computation.2 | convolution fusion | flops 2150105088 | bytes 9437184 | tf_op jit(solution)/shard_map/dot_general | solution.py:33
  74.4 5.2 %all-to-all-start.1 = ((bf16[16,32,2048]{2,1,0:T(8,128)(2,1)}), bf16[16,32,2048]{2,1,0:T(8,128)(2,1)}, u32[]{:S(2)}, u32[]{:S(2)}) async-start(bf16[16,32,2048]{2,1,0:T(8,128)(2,1)} %bitcast.43), calls=%async_computation.1 | async-start | bytes 4194304 | tf_op jit(solution)/shard_map/all_to_all | solution.py:35
  79.6 0.1 copy.13
  79.7 47.4 %all-to-all-done.1 = bf16[16,32,2048]{2,1,0:T(8,128)(2,1)} async-done(((bf16[16,32,2048]{2,1,0:T(8,128)(2,1)}), bf16[16,32,2048]{2,1,0:T(8,128)(2,1)}, u32[]{:S(2)}, u32[]{:S(2)}) %all-to-all-start.1) | async-done | bytes 2097184 | tf_op jit(solution)/shard_map/all_to_all | solution.py:35
  127.1 4.2 %gather_fusion = bf16[256,2048]{1,0:T(8,128)(2,1)S(1)} fusion(bf16[512,2048]{1,0:T(8,128)(2,1)} %bitcast.9, s32[1024]{0:T(1024)S(1)} %pad_clamp_fusion), kind=kCustom, calls=%fused_computation | custom fusion | bytes 2098176 | tf_op jit(solution)/shard_map/gather | solution.py:36
  131.3 2.4 %reshape.81 = f32[128,2,2048]{2,1,0:T(2,128)} reshape(bf16[256,2048]{1,0:T(8,128)(2,1)S(1)} %gather_fusion) | data formatting | bytes 3145728 | tf_op jit(solution)/shard_map/convert_element_type | solution.py:36
  133.7 5.6 %multiply_reduce_fusion = bf16[128,2048]{1,0:T(8,128)(2,1)} fusion(f32[128,2,2048]{2,1,0:T(2,128)} %reshape.81, f32[128,2]{1,0:T(8,128)S(1)} %copy.13), kind=kLoop, calls=%fused_computation.8 | loop fusion | flops 786432 | bytes 2622464 | tf_op jit(solution)/shard_map/reduce_sum | solution.py:38
  (13 shorter events, 0.1 us)
Async XLA Ops:
  0.0 68.3 %copy-start = (bf16[1,512,2048]{2,1,0:T(8,128)(2,1)S(1)}, bf16[1,512,2048]{2,1,0:T(8,128)(2,1)}, u32[]{:S(2)}) copy-start(bf16[1,512,2048]{2,1,0:T(8,128)(2,1)} %param.13) | copy-start | bytes 6291460
  11.9 55.2 %copy-start.3 = (bf16[1,2048,512]{2,1,0:T(8,128)(2,1)S(1)}, bf16[1,2048,512]{2,1,0:T(8,128)(2,1)}, u32[]{:S(2)}) copy-start(bf16[1,2048,512]{2,1,0:T(8,128)(2,1)} %param.11) | copy-start | bytes 6291460
  65.8 1.3 copy-start.1
  74.4 5.2 %copy-start.2 = (f32[128,2]{0,1:T(2,128)S(1)}, f32[128,2]{0,1:T(2,128)}, u32[]{:S(2)}) copy-start(f32[128,2]{0,1:T(2,128)} %param.9) | copy-start | bytes 3076
  74.4 52.7 %all-to-all-start.1 = ((bf16[16,32,2048]{2,1,0:T(8,128)(2,1)}), bf16[16,32,2048]{2,1,0:T(8,128)(2,1)}, u32[]{:S(2)}, u32[]{:S(2)}) async-start(bf16[16,32,2048]{2,1,0:T(8,128)(2,1)} %bitcast.43), calls=%async_computation.1 | async-start | bytes 4194304 | tf_op jit(solution)/shard_map/all_to_all | solution.py:35
where the time goes:
time: 140 us; the launch traced here: 139 us
  blocking collectives  53.9 us (38%)
  waiting for transfers between devices  47.4 us (34%)
  local copies, waits for them, and re-layouts  16 us (11%)
  other arithmetic  9.47 us (7%)
  matrix products  7.31 us (5%)
  starting transfers between devices  5.16 us (4%)
    all_to_all x1, blocking collectives, body(): lax.all_to_all(buffer, ('ep', 'tp'), split_axis=0, concat_axis=0, tiled=T...  53.9 us
    all_to_all x1, waiting for transfers between devices, body(): lax.all_to_all(results, ('ep', 'tp'), split_axis=0, concat_axis=0, tiled=...  47.4 us
    dot_general x1, matrix products, body(): jnp.dot(hidden, down_proj[0], preferred_element_type=jnp.float32)  6.06 us
    reduce_sum x1, other arithmetic, body(): jnp.sum(picked * route_weights[:, :, None], axis=1).astype(jnp.bfloat16)  5.59 us
    all_to_all x1, starting transfers between devices, body(): lax.all_to_all(results, ('ep', 'tp'), split_axis=0, concat_axis=0, tiled=...  5.16 us
    scatter x1, local copies, waits for them, and re-layouts, body(): jnp.zeros((expert_count * capacity, model_width), jnp.bfloat16).at[target]  4.43 us
    gather x1, local copies, waits for them, and re-layouts, body(): picked = returned.reshape(-1, model_width)[target].astype(jnp.float32)  4.22 us
  transfers between devices with their start and end apart: 1, of which 1 were waited for; matrix products, arithmetic and copies ran while one was open for 0% of the time, Pallas kernels for 0%

commit v1 on v0

--- a/solution.py
+++ b/solution.py
@@ -1,17 +1,416 @@
+import functools
+
 import jax
 import jax.numpy as jnp
 from jax import lax
+from jax.experimental import pallas as pl
+from jax.experimental.pallas import tpu as pltpu
 from jax.sharding import PartitionSpec as P
 
-
-def body(hidden_in, expert_ids, route_weights, norm_gain, gate_proj, up_proj, down_proj):
+CHUNKS = 4
+
+
+def slot_capacity(choose_count, token_count, expert_count):
+    return max(2, 2 * choose_count * token_count // expert_count)
+
+
+def pick(z, table):
+    value = jnp.int32(table[0])
+    for index in range(1, len(table)):
+        value = jnp.where(z == index, jnp.int32(table[index]), value)
+    return value
+
+
+def kernel(
+    n, m, cap, chunks,
+    hid, ids, wts, gain, gate_hbm, up_hbm, down_hbm, out,
+    ag, meta, disp, xin, res, back, part, rin_l, rin_r, acc, gate, up, down,
+    w_sem, ag_s, ag_r, me_s, me_r, xd_s, xd_r, xb_s, xb_r, rs_s, rs_l, rs_r,
+):
+    z = lax.axis_index("ep")
+    t = lax.axis_index("tp")
+    tokens, width = hid.shape
+    rows = m * cap
+    cw = width // chunks
+    choose = ids.shape[0]
+    experts = n * m
+    middle = jnp.logical_and(z > 0, z < n - 1)
+    end = jnp.logical_or(z == 0, z == n - 1)
+    by_z = [sorted(range(n), key=lambda b: (abs(b - q), b)) for q in range(n)]
+    order = [pick(z, [by_z[q][s] for q in range(n)]) for s in range(n)]
+
+    def to_ep(q):
+        return {"ep": q}
+
+    def to_tp(q):
+        return {"tp": q}
+
+    def cols(c):
+        return pl.ds(c * cw, cw)
+
+    loads = [
+        pltpu.make_async_copy(gate_hbm.at[0], gate, w_sem.at[0]),
+        pltpu.make_async_copy(up_hbm.at[0], up, w_sem.at[1]),
+        pltpu.make_async_copy(down_hbm.at[0], down, w_sem.at[2]),
+    ]
+    for load in loads:
+        load.start()
+
+    barrier = pltpu.get_barrier_semaphore()
+
+    def greet(q):
+        pl.semaphore_signal(
+            barrier, inc=1, device_id=q, device_id_type=pl.DeviceIdType.MESH
+        )
+
+    for d in range(1, m):
+        greet(to_tp(lax.rem(t + d, m)))
+
+    @pl.when(z > 0)
+    def _():
+        greet(to_ep(z - 1))
+
+    @pl.when(z < n - 1)
+    def _():
+        greet(to_ep(z + 1))
+
+    def remote(src, dst, s_sem, r_sem, dev):
+        return pltpu.make_async_remote_copy(
+            src_ref=src, dst_ref=dst, send_sem=s_sem, recv_sem=r_sem,
+            device_id=dev, device_id_type=pl.DeviceIdType.MESH,
+        )
+
+    right, left = jnp.minimum(z + 1, n - 1), jnp.maximum(z - 1, 0)
+
+    def ag_copy(b, c, side):
+        return remote(
+            ag.at[b, :, cols(c)], ag.at[b, :, cols(c)], ag_s.at[side, b, c], ag_r.at[b, c],
+            to_ep(left if side == 0 else right),
+        )
+
+    def me_copy(b, side):
+        return remote(
+            meta.at[b], meta.at[b], me_s.at[side, b], me_r.at[b],
+            to_ep(left if side == 0 else right),
+        )
+
+    def xd_copy(b, j, c):
+        return remote(
+            disp.at[b, j, :, cols(c)], xin.at[b, t, :, cols(c)], xd_s.at[b, j, c],
+            xd_r.at[b, t, c], to_tp(j),
+        )
+
+    def xd_from(b, j, c):
+        return remote(
+            disp.at[b, j, :, cols(c)], xin.at[b, j, :, cols(c)], xd_s.at[b, j, c],
+            xd_r.at[b, j, c], to_tp(j),
+        )
+
+    def xb_copy(b, j, c):
+        return remote(
+            res.at[b, j, :, cols(c)], back.at[b, t, :, cols(c)], xb_s.at[b, j, c],
+            xb_r.at[b, t, c], to_tp(j),
+        )
+
+    def xb_from(b, j, c):
+        return remote(
+            res.at[b, j, :, cols(c)], back.at[b, j, :, cols(c)], xb_s.at[b, j, c],
+            xb_r.at[b, j, c], to_tp(j),
+        )
+
+    def rs_copy(b, c, side):
+        return remote(
+            part.at[b, :, cols(c)], (rin_r if side == 0 else rin_l).at[b, :, cols(c)],
+            rs_s.at[b, c], (rs_r if side == 0 else rs_l).at[b, c],
+            to_ep(left if side == 0 else right),
+        )
+
+    def rs_send(b, c):
+        @pl.when(b > z)
+        def _():
+            rs_copy(b, c, 1).start()
+
+        @pl.when(b < z)
+        def _():
+            rs_copy(b, c, 0).start()
+
+    expert_row = lax.broadcasted_iota(jnp.int32, (experts, tokens), 0)
+    named = [(expert_row == ids[k : k + 1, :]).astype(jnp.float32) for k in range(choose)]
+    total = named[0]
+    for k in range(1, choose):
+        total = total + named[k]
+    before = (
+        lax.broadcasted_iota(jnp.int32, (tokens, tokens), 0)
+        < lax.broadcasted_iota(jnp.int32, (tokens, tokens), 1)
+    ).astype(jnp.bfloat16)
+    counts = jnp.dot(total.astype(jnp.bfloat16), before, preferred_element_type=jnp.float32)
+    first = expert_row.astype(jnp.float32) * cap + counts
+    lines = [jnp.sum(named[k] * first, axis=0, keepdims=True) for k in range(choose)]
+    lines += [wts[k : k + 1, :] for k in range(choose)]
+    lines.append(jnp.zeros((meta.shape[1] - 2 * choose, tokens), jnp.float32))
+    meta[z] = jnp.concatenate(lines, axis=0)
+
+    hidden = hid[...].astype(jnp.float32)
+    scale = lax.rsqrt(jnp.mean(hidden * hidden, axis=-1, keepdims=True) + 1e-06)
+    ag[z] = (hidden * scale * gain[...]).astype(jnp.bfloat16)
+
+    partners = (m - 1) + (z > 0).astype(jnp.int32) + (z < n - 1).astype(jnp.int32)
+    pl.semaphore_wait(barrier, partners)
+
+    @pl.when(z > 0)
+    def _():
+        me_copy(z, 0).start()
+
+    @pl.when(z < n - 1)
+    def _():
+        me_copy(z, 1).start()
+
+    for c in range(chunks):
+        @pl.when(z > 0)
+        def _(c=c):
+            ag_copy(z, c, 0).start()
+
+        @pl.when(z < n - 1)
+        def _(c=c):
+            ag_copy(z, c, 1).start()
+
+    def receive(b, c):
+        if c == 0:
+            me_copy(b, 0).wait_recv()
+        ag_copy(b, c, 0).wait_recv()
+
+    def forward(s):
+        b = order[s]
+
+        @pl.when(middle)
+        def _():
+            for c in range(chunks):
+                receive(b, c)
+
+                @pl.when(b < z)
+                def _(c=c):
+                    if c == 0:
+                        me_copy(b, 1).start()
+                    ag_copy(b, c, 1).start()
+
+                @pl.when(b > z)
+                def _(c=c):
+                    if c == 0:
+                        me_copy(b, 0).start()
+                    ag_copy(b, c, 0).start()
+
+    def slot_row():
+        row = lax.broadcasted_iota(jnp.int32, (rows, tokens), 0) + z * rows
+        return row.astype(jnp.float32)
+
+    def dispatch(s, wait):
+        b = order[s]
+        select = None
+        for c in range(chunks):
+            if wait:
+                receive(b, c)
+            if select is None:
+                info = meta[b]
+                row = slot_row()
+                select = jnp.zeros((rows, tokens), jnp.float32)
+                for k in range(choose):
+                    select = select + (row == info[k : k + 1, :]).astype(jnp.float32)
+                select = select.astype(jnp.bfloat16)
+            sent = jnp.dot(select, ag[b, :, cols(c)], preferred_element_type=jnp.float32)
+            disp[b, :, :, cols(c)] = sent.astype(jnp.bfloat16).reshape(m, cap, cw)
+            for d in range(m - 1, 0, -1):
+                xd_copy(b, lax.rem(t + d, m), c).start()
+            xin[b, t, :, cols(c)] = disp[b, t, :, cols(c)]
+
+    def experts_step(s):
+        b = order[s]
+        if s == 0:
+            loads[0].wait()
+            loads[1].wait()
+        gate_act = jnp.zeros((rows, gate.shape[1]), jnp.float32)
+        up_act = jnp.zeros((rows, gate.shape[1]), jnp.float32)
+        for c in range(chunks):
+            for d in range(1, m):
+                xd_from(b, lax.rem(t + d, m), c).wait_recv()
+            block = xin[b, :, :, cols(c)].reshape(rows, cw)
+            gate_act += jnp.dot(block, gate[cols(c), :], preferred_element_type=jnp.float32)
+            up_act += jnp.dot(block, up[cols(c), :], preferred_element_type=jnp.float32)
+        act = (gate_act / (1.0 + jnp.exp(-gate_act)) * up_act).astype(jnp.bfloat16)
+        if s == 0:
+            loads[2].wait()
+        for c in range(chunks):
+            made = jnp.dot(act, down[:, cols(c)], preferred_element_type=jnp.float32)
+            res[b, :, :, cols(c)] = made.astype(jnp.bfloat16).reshape(m, cap, cw)
+            for d in range(m - 1, 0, -1):
+                xb_copy(b, lax.rem(t + d, m), c).start()
+            back[b, t, :, cols(c)] = res[b, t, :, cols(c)]
+
+    def combine(s):
+        b = order[s]
+        info = meta[b]
+        row = slot_row()
+        mix = jnp.zeros((rows, tokens), jnp.float32)
+        for k in range(choose):
+            mix = mix + jnp.where(
+                row == info[k : k + 1, :], info[choose + k : choose + k + 1, :], 0.0
+            )
+        mix = jnp.transpose(mix).astype(jnp.bfloat16)
+        for c in range(chunks):
+            for d in range(1, m):
+                xb_from(b, lax.rem(t + d, m), c).wait_recv()
+            block = back[b, :, :, cols(c)].reshape(rows, cw)
+            value = jnp.dot(mix, block, preferred_element_type=jnp.float32)
+            if s == 0:
+                acc[:, cols(c)] = value
+            else:
+                part[b, :, cols(c)] = value.astype(jnp.bfloat16)
+
+                @pl.when(end)
+                def _(c=c):
+                    rs_send(b, c)
+
+    dispatch(0, False)
+    experts_step(0)
+    for s in (1, 2):
+        if s < n:
+            forward(s)
+
+    def ready(s, where):
+        if s < n:
+            @pl.when(where)
+            def _():
+                dispatch(s, where is end)
+
+    ready(1, middle)
+    ready(2, middle)
+    ready(1, end)
+    combine(0)
+    for s in range(1, n):
+        experts_step(s)
+        combine(s)
+        if s + 2 < n:
+            forward(s + 2)
+        ready(s + 2, middle)
+        ready(s + 1, end)
+
+    def due(q):
+        return sorted(
+            [b for b in range(n) if b != q],
+            key=lambda b: (b, q) if b > q else (n - 1 - b, n - 1 - q),
+        )
+
+    dues = [due(q) for q in range(n)]
+    later = [pick(z, [dues[q][s] for q in range(n)]) for s in range(n - 1)]
+
+    @pl.when(middle)
+    def _():
+        def add(b, c):
+            @pl.when(b > z)
+            def _():
+                rs_copy(b, c, 1).wait_recv()
+                part[b, :, cols(c)] = part[b, :, cols(c)] + rin_l[b, :, cols(c)]
+
+            @pl.when(b < z)
+            def _():
+                rs_copy(b, c, 0).wait_recv()
+                part[b, :, cols(c)] = part[b, :, cols(c)] + rin_r[b, :, cols(c)]
+
+            rs_send(b, c)
+
+        for b in later[:-2]:
+            for c in range(chunks):
+                add(b, c)
+        for c in range(chunks):
+            for b in later[-2:]:
+                add(b, c)
+
+    for c in range(chunks):
+        @pl.when(z > 0)
+        def _(c=c):
+            rs_copy(z, c, 1).wait_recv()
+            acc[:, cols(c)] = acc[:, cols(c)] + rin_l[z, :, cols(c)].astype(jnp.float32)
+
+        @pl.when(z < n - 1)
+        def _(c=c):
+            rs_copy(z, c, 0).wait_recv()
+            acc[:, cols(c)] = acc[:, cols(c)] + rin_r[z, :, cols(c)].astype(jnp.float32)
+
+        out[:, cols(c)] = acc[:, cols(c)].astype(jnp.bfloat16)
+
+    for s in range(n):
+        b = order[s]
+
+        @pl.when(jnp.logical_and(b >= z, z > 0))
+        def _(b=b):
+            me_copy(b, 0).wait_send()
+            for c in range(chunks):
+                ag_copy(b, c, 0).wait_send()
+
+        @pl.when(jnp.logical_and(b <= z, z < n - 1))
+        def _(b=b):
+            me_copy(b, 1).wait_send()
+            for c in range(chunks):
+                ag_copy(b, c, 1).wait_send()
+
+        for c in range(chunks):
+            for d in range(1, m):
+                xd_copy(b, lax.rem(t + d, m), c).wait_send()
+                xb_copy(b, lax.rem(t + d, m), c).wait_send()
+            if s > 0:
+                rs_copy(b, c, 0).wait_send()
+
+
+def fused(n, m, cap, hidden_in, expert_ids, route_weights, norm_gain, gate_proj, up_proj, down_proj):
+    tokens, width = hidden_in.shape
+    units = gate_proj.shape[2]
+    chunks = CHUNKS
+    choose = expert_ids.shape[1]
+    lines = -(-2 * choose // 8) * 8
+    bf = jnp.bfloat16
+    dma = pltpu.SemaphoreType.DMA
+    vmem = pl.BlockSpec(memory_space=pltpu.VMEM)
+    hbm = pl.BlockSpec(memory_space=pl.ANY)
+    return pl.pallas_call(
+        functools.partial(kernel, n, m, cap, chunks),
+        out_shape=jax.ShapeDtypeStruct((tokens, width), bf),
+        in_specs=[vmem] * 4 + [hbm] * 3,
+        out_specs=vmem,
+        scratch_shapes=[
+            pltpu.VMEM((n, tokens, width), bf),
+            pltpu.VMEM((n, lines, tokens), jnp.float32),
+            pltpu.VMEM((n, m, cap, width), bf),
+            pltpu.VMEM((n, m, cap, width), bf),
+            pltpu.VMEM((n, m, cap, width), bf),
+            pltpu.VMEM((n, m, cap, width), bf),
+            pltpu.VMEM((n, tokens, width), bf),
+            pltpu.VMEM((n, tokens, width), bf),
+            pltpu.VMEM((n, tokens, width), bf),
+            pltpu.VMEM((tokens, width), jnp.float32),
+            pltpu.VMEM((width, units), bf),
+            pltpu.VMEM((width, units), bf),
+            pltpu.VMEM((units, width), bf),
+            dma((3,)),
+            dma((2, n, chunks)), dma((n, chunks)),
+            dma((2, n)), dma((n,)),
+            dma((n, m, chunks)), dma((n, m, chunks)),
+            dma((n, m, chunks)), dma((n, m, chunks)),
+            dma((n, chunks)), dma((n, chunks)), dma((n, chunks)),
+        ],
+        compiler_params=pltpu.CompilerParams(
+            collective_id=0, has_side_effects=True, vmem_limit_bytes=48 * 1024 * 1024
+        ),
+        name="experts",
+    )(
+        hidden_in, expert_ids.T, route_weights.T, norm_gain.reshape(1, -1),
+        gate_proj, up_proj, down_proj,
+    )
+
+
+def by_slots(capacity, hidden_in, expert_ids, route_weights, norm_gain, gate_proj, up_proj, down_proj):
     token_count = hidden_in.shape[0]
     model_width = hidden_in.shape[1]
     choose_count = expert_ids.shape[1]
-    ep_count = lax.axis_size("ep")
-    tp_count = lax.axis_size("tp")
-    expert_count = ep_count * tp_count
-    capacity = max(2, 2 * choose_count * token_count // expert_count)
+    expert_count = lax.axis_size("ep") * lax.axis_size("tp")
     as_float = hidden_in.astype(jnp.float32)
     scaled = as_float * lax.rsqrt(jnp.mean(as_float * as_float, axis=-1, keepdims=True) + 1e-06)
     normed = (scaled * norm_gain).astype(jnp.bfloat16)
@@ -38,6 +437,15 @@
     return jnp.sum(picked * route_weights[:, :, None], axis=1).astype(jnp.bfloat16)
 
 
+def body(hidden_in, expert_ids, *rest):
+    n, m = lax.axis_size("ep"), lax.axis_size("tp")
+    tokens = hidden_in.shape[0]
+    cap = slot_capacity(expert_ids.shape[1], tokens, n * m)
+    if n > 2 and m * cap >= tokens and cap % 16 == 0:
+        return fused(n, m, cap, hidden_in, expert_ids, *rest)
+    return by_slots(cap, hidden_in, expert_ids, *rest)
+
+
 def solution(mesh):
     return jax.shard_map(
         body,

time: 140 us -> 101 us (0.72)
  the two profiles are of different devices: /device:TPU:11 before, /device:TPU:0 now
where the time goes in v1:
time: 101 us
  Pallas kernels  93.9 us (93%)
  local copies, waits for them, and re-layouts  7.07 us (7%)
    pallas_call x1, Pallas kernels, fused(): pl.pallas_call(functools.partial(kernel, n, m, cap, chunks), out_shape=ja...  93.9 us
    unnamed x13, local copies, waits for them, and re-layouts  7.07 us

profile of v1, /device:TPU:0, one launch (start us, length us, event | category | flops | bytes accessed | tf_op | source)
XLA Modules:
  0.0 101.0 jit_solution(12222947861222844885)
XLA Ops:
  0.0 0.0 copy-start
  0.0 1.6 %copy-done = bf16[1,2048,512]{2,1,0:T(8,128)(2,1)S(1)} copy-done((bf16[1,2048,512]{2,1,0:T(8,128)(2,1)S(1)}, bf16[1,2048,512]{2,1,0:T(8,128)(2,1)}, u32[]{:S(2)}) %copy-start) | copy-done | bytes 2097176
  1.6 0.0 copy-start.1
  1.6 1.6 %copy-done.1 = bf16[1,2048,512]{2,1,0:T(8,128)(2,1)S(1)} copy-done((bf16[1,2048,512]{2,1,0:T(8,128)(2,1)S(1)}, bf16[1,2048,512]{2,1,0:T(8,128)(2,1)}, u32[]{:S(2)}) %copy-start.1) | copy-done | bytes 2097176
  3.2 0.0 copy-start.2
  3.2 1.0 %copy-done.2 = bf16[128,2048]{1,0:T(8,128)(2,1)S(1)} copy-done((bf16[128,2048]{1,0:T(8,128)(2,1)S(1)}, bf16[128,2048]{1,0:T(8,128)(2,1)}, u32[]{:S(2)}) %copy-start.2) | copy-done | bytes 524312
  4.2 0.0 copy-start.3
  4.2 0.7 copy-done.3
  4.9 0.0 copy-start.4
  4.9 0.7 copy-done.4
  5.6 0.0 copy-start.5
  5.6 0.7 copy-done.5
  6.3 93.9 %experts.1 = bf16[128,2048]{1,0:T(8,128)(2,1)S(1)} custom-call(bf16[128,2048]{1,0:T(8,128)(2,1)S(1)} %copy-done.2, s32[2,128]{1,0:T(2,128)S(1)} %bitcast.4, f32[2,128]{1,0:T(2,128)S(1)} %bitcast.5, f32[1,2048]{1,0:T(1,128)S(1)} %bitcast.3, bf16[1,2048,512]{2,1,0:T(8,128)(2,1)S(1)} %copy-done, bf16[1,2048,512]{2,1,0:T(8,128)(2,1)S(1)} %copy-done.1, ...), custom_call_target="tpu_custom_call" | custom-call | tf_op jit(solution)/shard_map/experts/pallas_call | solution.py:373
  100.2 0.8 copy.9
Async XLA Ops:
  0.0 1.6 %copy-start = (bf16[1,2048,512]{2,1,0:T(8,128)(2,1)S(1)}, bf16[1,2048,512]{2,1,0:T(8,128)(2,1)}, u32[]{:S(2)}) copy-start(bf16[1,2048,512]{2,1,0:T(8,128)(2,1)} %gate_hbm.1) | copy-start | bytes 6291460
  1.6 1.6 %copy-start.1 = (bf16[1,2048,512]{2,1,0:T(8,128)(2,1)S(1)}, bf16[1,2048,512]{2,1,0:T(8,128)(2,1)}, u32[]{:S(2)}) copy-start(bf16[1,2048,512]{2,1,0:T(8,128)(2,1)} %up_hbm.1) | copy-start | bytes 6291460
  3.2 1.0 %copy-start.2 = (bf16[128,2048]{1,0:T(8,128)(2,1)S(1)}, bf16[128,2048]{1,0:T(8,128)(2,1)}, u32[]{:S(2)}) copy-start(bf16[128,2048]{1,0:T(8,128)(2,1)} %hid.1) | copy-start | bytes 1572868
  4.2 0.7 copy-start.3
  4.9 0.7 copy-start.4
  5.6 0.7 copy-start.5

commit v2 on v1

--- a/solution.py
+++ b/solution.py
@@ -7,7 +7,8 @@
 from jax.experimental.pallas import tpu as pltpu
 from jax.sharding import PartitionSpec as P
 
-CHUNKS = 4
+Z_CHUNKS = 2
+X_CHUNKS = 1
 
 
 def slot_capacity(choose_count, token_count, expert_count):
@@ -22,7 +23,7 @@
 
 
 def kernel(
-    n, m, cap, chunks,
+    n, m, cap, chunks, xchunks,
     hid, ids, wts, gain, gate_hbm, up_hbm, down_hbm, out,
     ag, meta, disp, xin, res, back, part, rin_l, rin_r, acc, gate, up, down,
     w_sem, ag_s, ag_r, me_s, me_r, xd_s, xd_r, xb_s, xb_r, rs_s, rs_l, rs_r,
@@ -32,6 +33,8 @@
     tokens, width = hid.shape
     rows = m * cap
     cw = width // chunks
+    xw = width // xchunks
+    ratio = chunks // xchunks
     choose = ids.shape[0]
     experts = n * m
     middle = jnp.logical_and(z > 0, z < n - 1)
@@ -47,6 +50,9 @@
 
     def cols(c):
         return pl.ds(c * cw, cw)
+
+    def xcols(q):
+        return pl.ds(q * xw, xw)
 
     loads = [
         pltpu.make_async_copy(gate_hbm.at[0], gate, w_sem.at[0]),
@@ -84,7 +90,7 @@
 
     def ag_copy(b, c, side):
         return remote(
-            ag.at[b, :, cols(c)], ag.at[b, :, cols(c)], ag_s.at[side, b, c], ag_r.at[b, c],
+            ag.at[b, c], ag.at[b, c], ag_s.at[side, b, c], ag_r.at[b, c],
             to_ep(left if side == 0 else right),
         )
 
@@ -96,31 +102,31 @@
 
     def xd_copy(b, j, c):
         return remote(
-            disp.at[b, j, :, cols(c)], xin.at[b, t, :, cols(c)], xd_s.at[b, j, c],
+            disp.at[b, c, j], xin.at[b, c, t], xd_s.at[b, j, c],
             xd_r.at[b, t, c], to_tp(j),
         )
 
     def xd_from(b, j, c):
         return remote(
-            disp.at[b, j, :, cols(c)], xin.at[b, j, :, cols(c)], xd_s.at[b, j, c],
+            disp.at[b, c, j], xin.at[b, c, j], xd_s.at[b, j, c],
             xd_r.at[b, j, c], to_tp(j),
         )
 
     def xb_copy(b, j, c):
         return remote(
-            res.at[b, j, :, cols(c)], back.at[b, t, :, cols(c)], xb_s.at[b, j, c],
+            res.at[b, c, j], back.at[b, c, t], xb_s.at[b, j, c],
             xb_r.at[b, t, c], to_tp(j),
         )
 
     def xb_from(b, j, c):
         return remote(
-            res.at[b, j, :, cols(c)], back.at[b, j, :, cols(c)], xb_s.at[b, j, c],
+            res.at[b, c, j], back.at[b, c, j], xb_s.at[b, j, c],
             xb_r.at[b, j, c], to_tp(j),
         )
 
     def rs_copy(b, c, side):
         return remote(
-            part.at[b, :, cols(c)], (rin_r if side == 0 else rin_l).at[b, :, cols(c)],
+            part.at[b, c], (rin_r if side == 0 else rin_l).at[b, c],
             rs_s.at[b, c], (rs_r if side == 0 else rs_l).at[b, c],
             to_ep(left if side == 0 else right),
         )
@@ -152,7 +158,9 @@
 
     hidden = hid[...].astype(jnp.float32)
     scale = lax.rsqrt(jnp.mean(hidden * hidden, axis=-1, keepdims=True) + 1e-06)
-    ag[z] = (hidden * scale * gain[...]).astype(jnp.bfloat16)
+    for c in range(chunks):
+        normed = hidden[:, c * cw : (c + 1) * cw] * scale * gain[:, cols(c)]
+        ag[z, c] = normed.astype(jnp.bfloat16)
 
     partners = (m - 1) + (z > 0).astype(jnp.int32) + (z < n - 1).astype(jnp.int32)
     pl.semaphore_wait(barrier, partners)
@@ -181,23 +189,20 @@
 
     def forward(s):
         b = order[s]
-
-        @pl.when(middle)
-        def _():
-            for c in range(chunks):
-                receive(b, c)
-
-                @pl.when(b < z)
-                def _(c=c):
-                    if c == 0:
-                        me_copy(b, 1).start()
-                    ag_copy(b, c, 1).start()
-
-                @pl.when(b > z)
-                def _(c=c):
-                    if c == 0:
-                        me_copy(b, 0).start()
-                    ag_copy(b, c, 0).start()
+        for c in range(chunks):
+            receive(b, c)
+
+            @pl.when(b < z)
+            def _(c=c):
+                if c == 0:
+                    me_copy(b, 1).start()
+                ag_copy(b, c, 1).start()
+
+            @pl.when(b > z)
+            def _(c=c):
+                if c == 0:
+                    me_copy(b, 0).start()
+                ag_copy(b, c, 0).start()
 
     def slot_row():
         row = lax.broadcasted_iota(jnp.int32, (rows, tokens), 0) + z * rows
@@ -216,11 +221,14 @@
                 for k in range(choose):
                     select = select + (row == info[k : k + 1, :]).astype(jnp.float32)
                 select = select.astype(jnp.bfloat16)
-            sent = jnp.dot(select, ag[b, :, cols(c)], preferred_element_type=jnp.float32)
-            disp[b, :, :, cols(c)] = sent.astype(jnp.bfloat16).reshape(m, cap, cw)
-            for d in range(m - 1, 0, -1):
-                xd_copy(b, lax.rem(t + d, m), c).start()
-            xin[b, t, :, cols(c)] = disp[b, t, :, cols(c)]
+            sent = jnp.dot(select, ag[b, c], preferred_element_type=jnp.float32)
+            q = c // ratio
+            inner = pl.ds((c % ratio) * cw, cw)
+            disp[b, q, :, :, inner] = sent.astype(jnp.bfloat16).reshape(m, cap, cw)
+            if (c + 1) % ratio == 0:
+                for d in range(m - 1, 0, -1):
+                    xd_copy(b, lax.rem(t + d, m), q).start()
+                xin[b, q, t] = disp[b, q, t]
 
     def experts_step(s):
         b = order[s]
@@ -229,21 +237,21 @@
             loads[1].wait()
         gate_act = jnp.zeros((rows, gate.shape[1]), jnp.float32)
         up_act = jnp.zeros((rows, gate.shape[1]), jnp.float32)
-        for c in range(chunks):
+        for q in range(xchunks):
             for d in range(1, m):
-                xd_from(b, lax.rem(t + d, m), c).wait_recv()
-            block = xin[b, :, :, cols(c)].reshape(rows, cw)
-            gate_act += jnp.dot(block, gate[cols(c), :], preferred_element_type=jnp.float32)
-            up_act += jnp.dot(block, up[cols(c), :], preferred_element_type=jnp.float32)
+                xd_from(b, lax.rem(t + d, m), q).wait_recv()
+            block = xin[b, q].reshape(rows, xw)
+            gate_act += jnp.dot(block, gate[xcols(q), :], preferred_element_type=jnp.float32)
+            up_act += jnp.dot(block, up[xcols(q), :], preferred_element_type=jnp.float32)
         act = (gate_act / (1.0 + jnp.exp(-gate_act)) * up_act).astype(jnp.bfloat16)
         if s == 0:
             loads[2].wait()
-        for c in range(chunks):
-            made = jnp.dot(act, down[:, cols(c)], preferred_element_type=jnp.float32)
-            res[b, :, :, cols(c)] = made.astype(jnp.bfloat16).reshape(m, cap, cw)
+        for q in range(xchunks):
+            made = jnp.dot(act, down[:, xcols(q)], preferred_element_type=jnp.float32)
+            res[b, q] = made.astype(jnp.bfloat16).reshape(m, cap, xw)
             for d in range(m - 1, 0, -1):
-                xb_copy(b, lax.rem(t + d, m), c).start()
-            back[b, t, :, cols(c)] = res[b, t, :, cols(c)]
+                xb_copy(b, lax.rem(t + d, m), q).start()
+            back[b, q, t] = res[b, q, t]
 
     def combine(s):
         b = order[s]
@@ -256,42 +264,48 @@
             )
         mix = jnp.transpose(mix).astype(jnp.bfloat16)
         for c in range(chunks):
-            for d in range(1, m):
-                xb_from(b, lax.rem(t + d, m), c).wait_recv()
-            block = back[b, :, :, cols(c)].reshape(rows, cw)
+            q = c // ratio
+            if c % ratio == 0:
+                for d in range(1, m):
+                    xb_from(b, lax.rem(t + d, m), q).wait_recv()
+            block = back[b, q, :, :, pl.ds((c % ratio) * cw, cw)].reshape(rows, cw)
             value = jnp.dot(mix, block, preferred_element_type=jnp.float32)
             if s == 0:
                 acc[:, cols(c)] = value
             else:
-                part[b, :, cols(c)] = value.astype(jnp.bfloat16)
+                part[b, c] = value.astype(jnp.bfloat16)
 
                 @pl.when(end)
-                def _(c=c):
+                def _(c=c, b=b):
                     rs_send(b, c)
 
     dispatch(0, False)
     experts_step(0)
-    for s in (1, 2):
-        if s < n:
-            forward(s)
-
-    def ready(s, where):
-        if s < n:
-            @pl.when(where)
-            def _():
-                dispatch(s, where is end)
-
-    ready(1, middle)
-    ready(2, middle)
-    ready(1, end)
-    combine(0)
-    for s in range(1, n):
-        experts_step(s)
-        combine(s)
-        if s + 2 < n:
-            forward(s + 2)
-        ready(s + 2, middle)
-        ready(s + 1, end)
+
+    @pl.when(end)
+    def _():
+        for s in range(1, n):
+            dispatch(s, True)
+            if s == 1:
+                combine(0)
+            experts_step(s)
+            combine(s)
+
+    @pl.when(middle)
+    def _():
+        forward(1)
+        forward(2)
+        dispatch(1, False)
+        dispatch(2, False)
+        combine(0)
+        for s in range(1, n):
+            experts_step(s)
+            if s + 2 < n:
+                forward(s + 2)
+                dispatch(s + 2, False)
+            if s > 1:
+                combine(s - 1)
+        combine(n - 1)
 
     def due(q):
         return sorted(
@@ -308,12 +322,12 @@
             @pl.when(b > z)
             def _():
                 rs_copy(b, c, 1).wait_recv()
-                part[b, :, cols(c)] = part[b, :, cols(c)] + rin_l[b, :, cols(c)]
+                part[b, c] = part[b, c] + rin_l[b, c]
 
             @pl.when(b < z)
             def _():
                 rs_copy(b, c, 0).wait_recv()
-                part[b, :, cols(c)] = part[b, :, cols(c)] + rin_r[b, :, cols(c)]
+                part[b, c] = part[b, c] + rin_r[b, c]
 
             rs_send(b, c)
 
@@ -328,12 +342,12 @@
         @pl.when(z > 0)
         def _(c=c):
             rs_copy(z, c, 1).wait_recv()
-            acc[:, cols(c)] = acc[:, cols(c)] + rin_l[z, :, cols(c)].astype(jnp.float32)
+            acc[:, cols(c)] = acc[:, cols(c)] + rin_l[z, c].astype(jnp.float32)
 
         @pl.when(z < n - 1)
         def _(c=c):
             rs_copy(z, c, 0).wait_recv()
-            acc[:, cols(c)] = acc[:, cols(c)] + rin_r[z, :, cols(c)].astype(jnp.float32)
+            acc[:, cols(c)] = acc[:, cols(c)] + rin_r[z, c].astype(jnp.float32)
 
         out[:, cols(c)] = acc[:, cols(c)].astype(jnp.bfloat16)
 
@@ -353,17 +367,19 @@
                 ag_copy(b, c, 1).wait_send()
 
         for c in range(chunks):
-            for d in range(1, m):
-                xd_copy(b, lax.rem(t + d, m), c).wait_send()
-                xb_copy(b, lax.rem(t + d, m), c).wait_send()
             if s > 0:
                 rs_copy(b, c, 0).wait_send()
+        for q in range(xchunks):
+            for d in range(1, m):
+                xd_copy(b, lax.rem(t + d, m), q).wait_send()
+                xb_copy(b, lax.rem(t + d, m), q).wait_send()
 
 
 def fused(n, m, cap, hidden_in, expert_ids, route_weights, norm_gain, gate_proj, up_proj, down_proj):
     tokens, width = hidden_in.shape
     units = gate_proj.shape[2]
-    chunks = CHUNKS
+    chunks, xchunks = Z_CHUNKS, X_CHUNKS
+    cw, xw = width // chunks, width // xchunks
     choose = expert_ids.shape[1]
     lines = -(-2 * choose // 8) * 8
     bf = jnp.bfloat16
@@ -371,20 +387,20 @@
     vmem = pl.BlockSpec(memory_space=pltpu.VMEM)
     hbm = pl.BlockSpec(memory_space=pl.ANY)
     return pl.pallas_call(
-        functools.partial(kernel, n, m, cap, chunks),
+        functools.partial(kernel, n, m, cap, chunks, xchunks),
         out_shape=jax.ShapeDtypeStruct((tokens, width), bf),
         in_specs=[vmem] * 4 + [hbm] * 3,
         out_specs=vmem,
         scratch_shapes=[
-            pltpu.VMEM((n, tokens, width), bf),
+            pltpu.VMEM((n, chunks, tokens, cw), bf),
             pltpu.VMEM((n, lines, tokens), jnp.float32),
-            pltpu.VMEM((n, m, cap, width), bf),
-            pltpu.VMEM((n, m, cap, width), bf),
-            pltpu.VMEM((n, m, cap, width), bf),
-            pltpu.VMEM((n, m, cap, width), bf),
-            pltpu.VMEM((n, tokens, width), bf),
-            pltpu.VMEM((n, tokens, width), bf),
-            pltpu.VMEM((n, tokens, width), bf),
+            pltpu.VMEM((n, xchunks, m, cap, xw), bf),
+            pltpu.VMEM((n, xchunks, m, cap, xw), bf),
+            pltpu.VMEM((n, xchunks, m, cap, xw), bf),
+            pltpu.VMEM((n, xchunks, m, cap, xw), bf),
+            pltpu.VMEM((n, chunks, tokens, cw), bf),
+            pltpu.VMEM((n, chunks, tokens, cw), bf),
+            pltpu.VMEM((n, chunks, tokens, cw), bf),
             pltpu.VMEM((tokens, width), jnp.float32),
             pltpu.VMEM((width, units), bf),
             pltpu.VMEM((width, units), bf),
@@ -392,8 +408,8 @@
             dma((3,)),
             dma((2, n, chunks)), dma((n, chunks)),
             dma((2, n)), dma((n,)),
-            dma((n, m, chunks)), dma((n, m, chunks)),
-            dma((n, m, chunks)), dma((n, m, chunks)),
+            dma((n, m, xchunks)), dma((n, m, xchunks)),
+            dma((n, m, xchunks)), dma((n, m, xchunks)),
             dma((n, chunks)), dma((n, chunks)), dma((n, chunks)),
         ],
         compiler_params=pltpu.CompilerParams(

time: 101 us -> 95.7 us (0.948)
  Pallas kernels: 93.9 us -> 88.3 us
    pallas_call x1, Pallas kernels: 93.9 us -> 88.3 us  [fused(): pl.pallas_call(functools.partial(kernel, n, m, cap, chunks, xchunks), out...]
where the time goes in v2:
time: 95.7 us; the launch traced here: 95.4 us
  Pallas kernels  88.3 us (92%)
  local copies, waits for them, and re-layouts  7.07 us (7%)
    pallas_call x1, Pallas kernels, fused(): pl.pallas_call(functools.partial(kernel, n, m, cap, chunks, xchunks), out...  88.3 us
    unnamed x13, local copies, waits for them, and re-layouts  7.07 us

profile of v2, /device:TPU:0, one launch (start us, length us, event | category | flops | bytes accessed | tf_op | source)
XLA Modules:
  0.0 95.4 jit_solution(16868800398922988526)
XLA Ops:
  0.0 0.0 copy-start
  0.0 1.6 %copy-done = bf16[1,2048,512]{2,1,0:T(8,128)(2,1)S(1)} copy-done((bf16[1,2048,512]{2,1,0:T(8,128)(2,1)S(1)}, bf16[1,2048,512]{2,1,0:T(8,128)(2,1)}, u32[]{:S(2)}) %copy-start) | copy-done | bytes 2097176
  1.6 0.0 copy-start.1
  1.6 1.6 %copy-done.1 = bf16[1,2048,512]{2,1,0:T(8,128)(2,1)S(1)} copy-done((bf16[1,2048,512]{2,1,0:T(8,128)(2,1)S(1)}, bf16[1,2048,512]{2,1,0:T(8,128)(2,1)}, u32[]{:S(2)}) %copy-start.1) | copy-done | bytes 2097176
  3.2 0.0 copy-start.2
  3.2 1.0 %copy-done.2 = bf16[128,2048]{1,0:T(8,128)(2,1)S(1)} copy-done((bf16[128,2048]{1,0:T(8,128)(2,1)S(1)}, bf16[128,2048]{1,0:T(8,128)(2,1)}, u32[]{:S(2)}) %copy-start.2) | copy-done | bytes 524312
  4.2 0.0 copy-start.3
  4.2 0.7 copy-done.3
  4.9 0.0 copy-start.4
  4.9 0.7 copy-done.4
  5.6 0.0 copy-start.5
  5.6 0.7 copy-done.5
  6.3 88.3 %experts.1 = bf16[128,2048]{1,0:T(8,128)(2,1)S(1)} custom-call(bf16[128,2048]{1,0:T(8,128)(2,1)S(1)} %copy-done.2, s32[2,128]{1,0:T(2,128)S(1)} %bitcast.4, f32[2,128]{1,0:T(2,128)S(1)} %bitcast.5, f32[1,2048]{1,0:T(1,128)S(1)} %bitcast.3, bf16[1,2048,512]{2,1,0:T(8,128)(2,1)S(1)} %copy-done, bf16[1,2048,512]{2,1,0:T(8,128)(2,1)S(1)} %copy-done.1, ...), custom_call_target="tpu_custom_call" | custom-call | tf_op jit(solution)/shard_map/experts/pallas_call | solution.py:389
  94.6 0.8 copy.9
Async XLA Ops:
  0.0 1.6 %copy-start = (bf16[1,2048,512]{2,1,0:T(8,128)(2,1)S(1)}, bf16[1,2048,512]{2,1,0:T(8,128)(2,1)}, u32[]{:S(2)}) copy-start(bf16[1,2048,512]{2,1,0:T(8,128)(2,1)} %gate_hbm.1) | copy-start | bytes 6291460
  1.6 1.6 %copy-start.1 = (bf16[1,2048,512]{2,1,0:T(8,128)(2,1)S(1)}, bf16[1,2048,512]{2,1,0:T(8,128)(2,1)}, u32[]{:S(2)}) copy-start(bf16[1,2048,512]{2,1,0:T(8,128)(2,1)} %up_hbm.1) | copy-start | bytes 6291460
  3.2 1.0 %copy-start.2 = (bf16[128,2048]{1,0:T(8,128)(2,1)S(1)}, bf16[128,2048]{1,0:T(8,128)(2,1)}, u32[]{:S(2)}) copy-start(bf16[128,2048]{1,0:T(8,128)(2,1)} %hid.1) | copy-start | bytes 1572868
  4.2 0.7 copy-start.3
  4.9 0.7 copy-start.4
  5.6 0.7 copy-start.5
